TPU v7x, 32 devices: a whole 2x2x4 slice. The times are simulated.
32 devices in a mesh: rep: 4 (over z), fs: 4 (over y, x), tp: 2 (over core).
Axes of the slice: x: 2, y: 2, z: 4, core: 2. Of those that a mesh axis runs over, the one named last changes fastest.
Arguments:
- hidden_in: bfloat16 [2048, 2048], P('rep'), may hold values from -6 to 6
- cotangent: bfloat16 [2048, 2048], P('rep'), may hold values from -3 to 3
- w_up: bfloat16 [2048, 8192], P('rep', ('fs', 'tp')), may hold values from -0.125 to 0.125
- w_down: bfloat16 [8192, 2048], P(('fs', 'tp'), 'rep'), may hold values from -0.0625 to 0.0625
Outputs:
- input_grad: bfloat16 [2048, 2048], P('rep')
- up_grad: float32 [2048, 8192], P('rep', ('fs', 'tp'))
- down_grad: float32 [8192, 2048], P(('fs', 'tp'), 'rep')
All inputs are finite; a program needn't handle non-finite values.
Results may differ from a plain program's by a relative error of at most 0.017.
Values may be sent and summed in bfloat16 or wider, within the bound.
A program may use at most 64 MiB of HBM per device.

v0:
```python
import jax
import jax.numpy as jnp
from jax import lax
from jax.sharding import PartitionSpec as P


def contract_last(left, right):
    return lax.dot_general(
        left, right, (((1,), (1,)), ((), ())), preferred_element_type=jnp.float32
    )


def contract_first(left, right):
    return lax.dot_general(
        left, right, (((0,), (0,)), ((), ())), preferred_element_type=jnp.float32
    )


def on_device(hidden_in, cotangent, w_up, w_down):
    up_full = lax.all_gather(w_up, "rep", axis=0, tiled=True)
    back_grad = contract_last(cotangent, lax.all_gather(w_down, "rep", axis=1, tiled=True))
    preact = jnp.dot(hidden_in, up_full, preferred_element_type=jnp.float32)
    active = jnp.maximum(preact, 0.0)
    hidden = (active * active).astype(jnp.bfloat16)
    slopes = (2.0 * active * back_grad).astype(jnp.bfloat16)
    grad_upper = lax.psum_scatter(
        contract_first(hidden_in, slopes).astype(jnp.bfloat16),
        "rep",
        scatter_dimension=0,
        tiled=True,
    ).astype(jnp.float32)
    lower_rows = lax.psum_scatter(
        contract_first(cotangent, hidden).astype(jnp.bfloat16),
        "rep",
        scatter_dimension=0,
        tiled=True,
    ).astype(jnp.float32)
    down_grad = lower_rows.T
    partial_sum = contract_last(slopes, up_full).astype(jnp.bfloat16)
    input_grad = lax.psum(partial_sum, ("fs", "tp")).astype(jnp.float32).astype(jnp.bfloat16)
    return (input_grad, grad_upper, down_grad)


def solution(mesh):
    return jax.shard_map(
        on_device,
        mesh=mesh,
        in_specs=(P("rep", None), P("rep", None), P("rep", ("fs", "tp")), P(("fs", "tp"), "rep")),
        out_specs=(P("rep", None), P("rep", ("fs", "tp")), P(("fs", "tp"), "rep")),
        check_vma=False,
    )
```

profile of v0, /device:TPU:0, one launch (start us, length us, event | category | flops | bytes accessed | tf_op | source)
XLA Modules:
  0.0 414.7 jit_solution(14841434194789787365)
XLA Ops:
  7.2 0.0 copy-start
  7.2 0.0 all-gather.3.cloned.1.call-start
  7.2 0.7 all-gather.3.cloned.1.call-update
  7.9 0.0 all-gather.5.cloned.1.call-start
  8.0 0.7 all-gather.5.cloned.1.call-update
  8.7 0.0 reduce-scatter.3.cloned.1.call-start
  8.7 84.3 %all-gather.3.cloned.1.call-done = bf16[2048,1024]{1,0:T(8,128)(2,1)} async-done(((bf16[512,1024]{1,0:T(8,128)(2,1)}), bf16[2048,1024]{1,0:T(8,128)(2,1)}) %all-gather.3.cloned.1.call-update) | async-done | bytes 4194320 | tf_op jit(solution)/shard_map/all_gather | solution.py:20
  93.1 0.0 copy-done
  93.1 5.8 %fusion.2 = f32[512,1024]{1,0:T(8,128)} fusion(bf16[512,2048]{1,0:T(8,128)(2,1)S(1)} %copy-done, bf16[2048,1024]{1,0:T(8,128)(2,1)} %all-gather.3.cloned.1.call-done), kind=kOutput, calls=%fused_computation.8 | convolution fusion | flops 2147483648 | bytes 8388608 | tf_op jit(solution)/shard_map/dot_general | solution.py:22
  98.9 75.0 %all-gather.5.cloned.1.call-done = bf16[1024,2048]{1,0:T(8,128)(2,1)} async-done(((bf16[1024,512]{1,0:T(8,128)(2,1)}), bf16[1024,2048]{1,0:T(8,128)(2,1)}) %all-gather.5.cloned.1.call-update) | async-done | bytes 4194320 | tf_op jit(solution)/shard_map/all_gather | solution.py:21
  173.9 5.8 %multiply_convert_fusion.1 = bf16[512,1024]{1,0:T(8,128)(2,1)S(1)} fusion(f32[512,1024]{1,0:T(8,128)} %fusion.2, bf16[512,2048]{1,0:T(8,128)(2,1)} %param.5, bf16[1024,2048]{1,0:T(8,128)(2,1)} %all-gather.5.cloned.1.call-done), kind=kOutput, calls=%fused_computation.5 | convolution fusion | flops 2149580800 | bytes 9437184 | tf_op jit(solution)/shard_map/dot_general | solution.py:8
  179.7 4.4 %convert_bitcast_fusion.1 = bf16[2048,1024]{0,1:T(8,128)(2,1)} fusion(bf16[512,1024]{1,0:T(8,128)(2,1)S(1)} %multiply_convert_fusion.1, bf16[512,2048]{1,0:T(8,128)(2,1)S(1)} %copy-done), kind=kOutput, calls=%fused_computation.1 | convolution fusion | flops 2149580800 | bytes 7340032 | tf_op jit(solution)/shard_map/dot_general | solution.py:14
  184.1 0.0 reduce-scatter.3.cloned.1.call-update
  184.1 0.0 reduce-scatter.5.cloned.1.call-start
  184.2 6.6 %convert_bitcast_fusion = bf16[2048,1024]{0,1:T(8,128)(2,1)} fusion(bf16[512,2048]{1,0:T(8,128)(2,1)} %param.5, f32[512,1024]{1,0:T(8,128)} %fusion.2), kind=kOutput, calls=%fused_computation | convolution fusion | flops 2151153664 | bytes 8388608 | tf_op jit(solution)/shard_map/dot_general | solution.py:14
  190.8 0.0 reduce-scatter.5.cloned.1.call-update
  190.8 0.0 all-reduce.2.cloned.1.call-start
  190.8 5.9 %convolution_convert_fusion = bf16[512,2048]{1,0:T(8,128)(2,1)} fusion(bf16[512,1024]{1,0:T(8,128)(2,1)S(1)} %multiply_convert_fusion.1, bf16[2048,1024]{1,0:T(8,128)(2,1)} %all-gather.3.cloned.1.call-done), kind=kOutput, calls=%fused_computation.2 | convolution fusion | flops 2148532224 | bytes 7340032 | tf_op jit(solution)/shard_map/dot_general | solution.py:8
  196.7 0.0 all-reduce.2.cloned.1.call-update
  196.7 62.8 %reduce-scatter.3.cloned.1.call-done = bf16[512,1024]{0,1:T(8,128)(2,1)} async-done(((bf16[2048,1024]{0,1:T(8,128)(2,1)}), bf16[512,1024]{0,1:T(8,128)(2,1)}) %reduce-scatter.3.cloned.1.call-update) | async-done | bytes 1048592 | tf_op jit(solution)/shard_map/reduce_scatter | solution.py:26
  259.6 2.6 copy.7
  262.1 76.9 %reduce-scatter.5.cloned.1.call-done = bf16[512,1024]{0,1:T(8,128)(2,1)} async-done(((bf16[2048,1024]{0,1:T(8,128)(2,1)}), bf16[512,1024]{0,1:T(8,128)(2,1)}) %reduce-scatter.5.cloned.1.call-update) | async-done | bytes 1048592 | tf_op jit(solution)/shard_map/reduce_scatter | solution.py:32
  339.1 2.8 convert_bitcast_fusion.2
  341.9 63.1 %all-reduce.2.cloned.1.call-done = bf16[512,2048]{1,0:T(8,128)(2,1)} async-done(((bf16[512,2048]{1,0:T(8,128)(2,1)}), bf16[512,2048]{1,0:T(8,128)(2,1)}) %all-reduce.2.cloned.1.call-update) | async-done | bytes 2097168 | tf_op jit(solution)/shard_map/psum | solution.py:40
  405.0 3.2 copy.9
Async XLA Ops:
  7.2 85.9 %copy-start = (bf16[512,2048]{1,0:T(8,128)(2,1)S(1)}, bf16[512,2048]{1,0:T(8,128)(2,1)}, u32[]{:S(2)}) copy-start(bf16[512,2048]{1,0:T(8,128)(2,1)} %param.4) | copy-start | bytes 6291460
  7.2 85.9 %all-gather.3.cloned.1.call-start = ((), (), s32[]{:S(2)}) async-start(), calls=%async_computation.2 | async-start | bytes 5242880 | tf_op jit(solution)/shard_map/all_gather | solution.py:20
  7.9 166.0 %all-gather.5.cloned.1.call-start = ((), (), s32[]{:S(2)}) async-start(), calls=%async_computation.3 | async-start | bytes 5242880 | tf_op jit(solution)/shard_map/all_gather | solution.py:21
  8.7 250.9 %reduce-scatter.3.cloned.1.call-start = ((), (), s32[]{:S(2)}) async-start(), calls=%async_computation.5 | async-start | bytes 5242880 | tf_op jit(solution)/shard_map/reduce_scatter | solution.py:26
  184.1 154.9 %reduce-scatter.5.cloned.1.call-start = ((), (), s32[]{:S(2)}) async-start(), calls=%async_computation.6 | async-start | bytes 5242880 | tf_op jit(solution)/shard_map/reduce_scatter | solution.py:32
  190.8 214.2 %all-reduce.2.cloned.1.call-start = ((), (), s32[]{:S(2)}) async-start(), calls=%async_computation.4 | async-start | bytes 4194304 | tf_op jit(solution)/shard_map/psum | solution.py:40
Sparse Core Ops, SparseCore 0:
  9.6 83.4 all-gather.2
  94.6 79.2 all-gather.4
  184.3 75.2 reduce-scatter.2
  261.7 77.2 reduce-scatter.4
  342.7 62.2 all-reduce.1
where the time goes:
time: 415 us
  waiting for transfers between devices  364 us (88%)
  matrix products  28.5 us (7%)
  between operations  13.8 us (3%)
  local copies, waits for them, and re-layouts  5.73 us (1%)
    all_gather x1, waiting for transfers between devices, on_device(): up_full = lax.all_gather(w_up, 'rep', axis=0, tiled=True)  84.3 us
    reduce_scatter x1, waiting for transfers between devices, on_device(): lax.psum_scatter(contract_first(cotangent, hidden).astype(jnp.bfloat16),...  76.9 us
    all_gather x1, waiting for transfers between devices, on_device(): lax.all_gather(w_down, 'rep', axis=1, tiled=True)  75 us
    psum x1, waiting for transfers between devices, on_device(): lax.psum(partial_sum, ('fs', 'tp')).astype(jnp.float32).astype(jnp.bfloat16)  63.1 us
    reduce_scatter x1, waiting for transfers between devices, on_device(): lax.psum_scatter(contract_first(hidden_in, slopes).astype(jnp.bfloat16),...  62.8 us
    dot_general x2, matrix products, contract_last(): lax.dot_general(left, right, (((1,), (1,)), ((), ())), preferred_element_...  11.7 us
    dot_general x2, matrix products, contract_first(): lax.dot_general(left, right, (((0,), (0,)), ((), ())), preferred_element_...  10.9 us
  transfers between devices with their start and end apart: 5, of which 5 were waited for; matrix products, arithmetic and copies ran while one was open for 6% of the time, Pallas kernels for 0%

commit v1 on v0

--- a/solution.py
+++ b/solution.py
@@ -37,7 +37,9 @@
     ).astype(jnp.float32)
     down_grad = lower_rows.T
     partial_sum = contract_last(slopes, up_full).astype(jnp.bfloat16)
-    input_grad = lax.psum(partial_sum, ("fs", "tp")).astype(jnp.float32).astype(jnp.bfloat16)
+    input_grad = (
+        lax.psum(lax.psum(partial_sum, "fs"), "tp").astype(jnp.float32).astype(jnp.bfloat16)
+    )
     return (input_grad, grad_upper, down_grad)
 
 

time: 415 us -> 444 us (1.070)
  waiting for transfers between devices: 364 us -> 395 us
    reduce_scatter x1, waiting for transfers between devices: 62.8 us -> 79 us  [on_device(): lax.psum_scatter(contract_first(hidden_in, slopes).astype(jnp.bfloat16),...]
    psum x1 -> x2, waiting for transfers between devices: 63.1 us -> 78.1 us  [the longest x1 56.9 us: on_device(): lax.psum(partial_sum, 'fs')]
  transfers between devices with their start and end apart: 5 -> 6, of which waited for: 5 -> 6; matrix products, arithmetic and copies ran while one was open for 6% -> 5% of each run, Pallas kernels for 0% -> 0%
where the time goes in v1:
time: 444 us
  waiting for transfers between devices  395 us (89%)
  matrix products  26.6 us (6%)
  between operations  14.1 us (3%)
  local copies, waits for them, and re-layouts  5.73 us (1%)
    all_gather x1, waiting for transfers between devices, on_device(): up_full = lax.all_gather(w_up, 'rep', axis=0, tiled=True)  84.3 us
    reduce_scatter x1, waiting for transfers between devices, on_device(): lax.psum_scatter(contract_first(hidden_in, slopes).astype(jnp.bfloat16),...  79 us
    reduce_scatter x1, waiting for transfers between devices, on_device(): lax.psum_scatter(contract_first(cotangent, hidden).astype(jnp.bfloat16),...  76.9 us
    all_gather x1, waiting for transfers between devices, on_device(): lax.all_gather(w_down, 'rep', axis=1, tiled=True)  75 us
    psum x1, waiting for transfers between devices, on_device(): lax.psum(partial_sum, 'fs')  56.9 us
    psum x1, waiting for transfers between devices, on_device(): lax.psum(lax.psum(partial_sum, 'fs'), 'tp').astype(jnp.float32)  21.2 us
    dot_general x2, matrix products, contract_first(): lax.dot_general(left, right, (((0,), (0,)), ((), ())), preferred_element_...  11.1 us
    dot_general x2, matrix products, contract_last(): lax.dot_general(left, right, (((1,), (1,)), ((), ())), preferred_element_...  9.71 us
  transfers between devices with their start and end apart: 6, of which 6 were waited for; matrix products, arithmetic and copies ran while one was open for 5% of the time, Pallas kernels for 0%

profile of v1, /device:TPU:0, one launch (start us, length us, event | category | flops | bytes accessed | tf_op | source)
XLA Modules:
  0.0 444.2 jit_solution(6530498268015607381)
XLA Ops:
  7.2 0.0 copy-start
  7.2 0.0 all-gather.3.cloned.1.call-start
  7.2 0.7 all-gather.3.cloned.1.call-update
  7.9 0.0 all-gather.5.cloned.1.call-start
  8.0 0.7 all-gather.5.cloned.1.call-update
  8.7 0.0 all-reduce.3.cloned.1.call-start
  8.7 84.3 %all-gather.3.cloned.1.call-done = bf16[2048,1024]{1,0:T(8,128)(2,1)} async-done(((bf16[512,1024]{1,0:T(8,128)(2,1)}), bf16[2048,1024]{1,0:T(8,128)(2,1)}) %all-gather.3.cloned.1.call-update) | async-done | bytes 4194320 | tf_op jit(solution)/shard_map/all_gather | solution.py:20
  93.1 0.0 copy-done
  93.1 5.8 %fusion.2 = f32[512,1024]{1,0:T(8,128)} fusion(bf16[512,2048]{1,0:T(8,128)(2,1)S(1)} %copy-done, bf16[2048,1024]{1,0:T(8,128)(2,1)} %all-gather.3.cloned.1.call-done), kind=kOutput, calls=%fused_computation.8 | convolution fusion | flops 2147483648 | bytes 8388608 | tf_op jit(solution)/shard_map/dot_general | solution.py:22
  98.9 75.0 %all-gather.5.cloned.1.call-done = bf16[1024,2048]{1,0:T(8,128)(2,1)} async-done(((bf16[1024,512]{1,0:T(8,128)(2,1)}), bf16[1024,2048]{1,0:T(8,128)(2,1)}) %all-gather.5.cloned.1.call-update) | async-done | bytes 4194320 | tf_op jit(solution)/shard_map/all_gather | solution.py:21
  173.9 0.0 copy-start.1
  173.9 6.0 %multiply_convert_fusion.1 = bf16[512,1024]{1,0:T(8,128)(2,1)S(1)} fusion(f32[512,1024]{1,0:T(8,128)} %fusion.2, bf16[512,2048]{1,0:T(8,128)(2,1)} %param.5, bf16[1024,2048]{1,0:T(8,128)(2,1)} %all-gather.5.cloned.1.call-done), kind=kOutput, calls=%fused_computation.5 | convolution fusion | flops 2149580800 | bytes 9437184 | tf_op jit(solution)/shard_map/dot_general | solution.py:8
  179.9 0.0 copy-done.1
  179.9 3.7 convolution_convert_fusion
  183.6 0.0 all-reduce.3.cloned.1.call-update
  183.6 0.0 reduce-scatter.3.cloned.1.call-start
  183.7 4.5 %convert_bitcast_fusion.1 = bf16[2048,1024]{0,1:T(8,128)(2,1)} fusion(bf16[512,1024]{1,0:T(8,128)(2,1)S(1)} %multiply_convert_fusion.1, bf16[512,2048]{1,0:T(8,128)(2,1)S(1)} %copy-done), kind=kOutput, calls=%fused_computation.1 | convolution fusion | flops 2149580800 | bytes 7340032 | tf_op jit(solution)/shard_map/dot_general | solution.py:14
  188.2 0.0 reduce-scatter.3.cloned.1.call-update
  188.2 0.0 reduce-scatter.5.cloned.1.call-start
  188.2 6.6 %convert_bitcast_fusion = bf16[2048,1024]{0,1:T(8,128)(2,1)} fusion(bf16[512,2048]{1,0:T(8,128)(2,1)} %param.5, f32[512,1024]{1,0:T(8,128)} %fusion.2), kind=kOutput, calls=%fused_computation | convolution fusion | flops 2151153664 | bytes 8388608 | tf_op jit(solution)/shard_map/dot_general | solution.py:14
  194.8 0.0 reduce-scatter.5.cloned.1.call-update
  194.8 0.0 all-reduce.5.cloned.1.call-start
  194.9 56.9 %all-reduce.3.cloned.1.call-done = bf16[512,2048]{1,0:T(8,128)(2,1)} async-done(((bf16[512,2048]{1,0:T(8,128)(2,1)}), bf16[512,2048]{1,0:T(8,128)(2,1)}) %all-reduce.3.cloned.1.call-update) | async-done | bytes 2097168 | tf_op jit(solution)/shard_map/psum | solution.py:41
  251.8 0.0 all-reduce.5.cloned.1.call-update
  251.8 79.0 %reduce-scatter.3.cloned.1.call-done = bf16[512,1024]{0,1:T(8,128)(2,1)} async-done(((bf16[2048,1024]{0,1:T(8,128)(2,1)}), bf16[512,1024]{0,1:T(8,128)(2,1)}) %reduce-scatter.3.cloned.1.call-update) | async-done | bytes 1048592 | tf_op jit(solution)/shard_map/reduce_scatter | solution.py:26
  330.7 2.6 copy.7
  333.3 76.9 %reduce-scatter.5.cloned.1.call-done = bf16[512,1024]{0,1:T(8,128)(2,1)} async-done(((bf16[2048,1024]{0,1:T(8,128)(2,1)}), bf16[512,1024]{0,1:T(8,128)(2,1)}) %reduce-scatter.5.cloned.1.call-update) | async-done | bytes 1048592 | tf_op jit(solution)/shard_map/reduce_scatter | solution.py:32
  410.2 2.8 convert_bitcast_fusion.2
  413.0 21.2 %all-reduce.5.cloned.1.call-done = bf16[512,2048]{1,0:T(8,128)(2,1)} async-done(((bf16[512,2048]{1,0:T(8,128)(2,1)}), bf16[512,2048]{1,0:T(8,128)(2,1)}) %all-reduce.5.cloned.1.call-update) | async-done | bytes 2097168 | tf_op jit(solution)/shard_map/psum | solution.py:41
  434.2 3.2 copy.10
Async XLA Ops:
  7.2 85.9 %copy-start = (bf16[512,2048]{1,0:T(8,128)(2,1)S(1)}, bf16[512,2048]{1,0:T(8,128)(2,1)}, u32[]{:S(2)}) copy-start(bf16[512,2048]{1,0:T(8,128)(2,1)} %param.4) | copy-start | bytes 6291460
  7.2 85.9 %all-gather.3.cloned.1.call-start = ((), (), s32[]{:S(2)}) async-start(), calls=%async_computation.2 | async-start | bytes 5242880 | tf_op jit(solution)/shard_map/all_gather | solution.py:20
  7.9 166.0 %all-gather.5.cloned.1.call-start = ((), (), s32[]{:S(2)}) async-start(), calls=%async_computation.3 | async-start | bytes 5242880 | tf_op jit(solution)/shard_map/all_gather | solution.py:21
  8.7 243.1 %all-reduce.3.cloned.1.call-start = ((), (), s32[]{:S(2)}) async-start(), calls=%async_computation.4 | async-start | bytes 4194304 | tf_op jit(solution)/shard_map/psum | solution.py:41
  173.9 6.0 %copy-start.1 = (bf16[2048,1024]{1,0:T(8,128)(2,1)S(1)}, bf16[2048,1024]{1,0:T(8,128)(2,1)}, u32[]{:S(2)}) copy-start(bf16[2048,1024]{1,0:T(8,128)(2,1)} %all-gather.3.cloned.1.call-done) | copy-start | bytes 12582916
  183.6 147.1 %reduce-scatter.3.cloned.1.call-start = ((), (), s32[]{:S(2)}) async-start(), calls=%async_computation.6 | async-start | bytes 5242880 | tf_op jit(solution)/shard_map/reduce_scatter | solution.py:26
  188.2 222.0 %reduce-scatter.5.cloned.1.call-start = ((), (), s32[]{:S(2)}) async-start(), calls=%async_computation.7 | async-start | bytes 5242880 | tf_op jit(solution)/shard_map/reduce_scatter | solution.py:32
  194.8 239.4 %all-reduce.5.cloned.1.call-start = ((), (), s32[]{:S(2)}) async-start(), calls=%async_computation.5 | async-start | bytes 4194304 | tf_op jit(solution)/shard_map/psum | solution.py:41
Sparse Core Ops, SparseCore 0:
  9.6 83.4 all-gather.2
  94.6 79.2 all-gather.4
  183.8 67.9 all-reduce.2
  253.9 76.7 reduce-scatter.2
  332.9 77.2 reduce-scatter.4
  412.4 21.7 all-reduce.4
